TPU v7x, 256 devices: a 8x8x2 block of a 8x8x16 slice. The times are simulated.
256 devices in a mesh: grp: 2 (over z), ep: 64 (over y, x), tp: 2 (over core).
Axes of the slice: x: 8, y: 8, z: 2, core: 2. Of those that a mesh axis runs over, the one named last changes fastest.
The devices are a block of a 8x8x16 slice.
Arguments:
- tokens: bfloat16 [65536, 2048], P(('grp', 'ep'), 'tp'), parts along dimension 0, may hold values from -6 to 6
- norm_gain: float32 [2048], replicated, may hold values from 0.1 to 1.9
- expert_ids: int32 [65536, 2], P(('grp', 'ep')), parts along dimension 0, may hold values from 0 to 63, all different within a row; in each aligned block of 512 rows (0 to 511, 512 to 1023, ...) at most 24 rows name the same one
- route_weights: float32 [65536, 2], P(('grp', 'ep')), parts along dimension 0, may hold values from 0.1 to 1
- gate_weight: bfloat16 [64, 2048, 512], P('ep', None, 'tp'), may hold values from -0.125 to 0.125
- up_weight: bfloat16 [64, 2048, 512], P('ep', None, 'tp'), may hold values from -0.125 to 0.125
- down_weight: bfloat16 [64, 512, 2048], P('ep', None, 'tp'), may hold values from -0.25 to 0.25
Outputs:
- mixed: bfloat16 [65536, 2048], P(('grp', 'ep'), 'tp'), parts along dimension 0
There are 2 independent parts, one for each index of `grp`. A program takes and returns all parts, laid end to end along the dimension named above; an argument that names none is the same for every part. Nothing has to cross between parts.
Inputs may be any that keep to these rules, and one draw needn't show every extreme that they name: `expert_ids`: each token names 2 different experts. Among the 512 tokens of one index of ep (aligned blocks of rows) at most 24 name the same expert, and in some block some expert is named by exactly 24 of them.
All inputs are finite; a program needn't handle non-finite values.
Results may differ from a plain program's by a relative error of at most 0.007.
Values may be sent and summed in bfloat16 or wider, within the bound.
A program may use at most 64 MiB of HBM per device.

v0:
```python
import jax
import jax.numpy as jnp
from jax import lax
from jax.sharding import PartitionSpec as P


def copy_for_each(array, axis):
    copies = jnp.broadcast_to(array, (lax.axis_size(axis), *array.shape))
    return lax.all_to_all(copies, axis, split_axis=0, concat_axis=0, tiled=True)


def joined_along(pieces, dim):
    lengths = list(pieces.shape[1:])
    lengths[dim] *= pieces.shape[0]
    return jnp.moveaxis(pieces, 0, dim).reshape(lengths)


def collect(array, axis, dim):
    pieces = copy_for_each(array, axis)
    return joined_along(pieces, dim)


def cut_along(array, dim, peers):
    lengths = array.shape
    pieces = array.reshape(*lengths[:dim], peers, lengths[dim] // peers, *lengths[dim + 1 :])
    return jnp.moveaxis(pieces, dim, 0)


def cut_rows(length, count):
    turn = length // count
    if turn >= 8:
        turn -= turn % 8
    return [turn * k for k in range(1, count)]


def cut_exchange(array, axis, pieces, split_dim, concat_dim):
    blocks = cut_along(array, split_dim, lax.axis_size(axis))
    split_at = max(range(1, max(2, blocks.ndim - 1)), key=lambda d: blocks.shape[d])
    finished = []
    for section in jnp.split(blocks, cut_rows(blocks.shape[split_at], pieces), axis=split_at):
        if section.size:
            finished.append(lax.all_to_all(section, axis, split_axis=0, concat_axis=0, tiled=True))
    return joined_along(jnp.concatenate(finished, axis=split_at), concat_dim)


def normalize(rows, norm_gain):
    xf = rows.astype(jnp.float32)
    scale = lax.rsqrt(jnp.mean(xf * xf, axis=-1, keepdims=True) + 1e-06)
    return (xf * scale * norm_gain[None, :]).astype(jnp.bfloat16)


def on_device(tokens, norm_gain, expert_ids, route_weights, gate_weight, up_weight, down_weight):
    tok_rows, half = tokens.shape
    width = half * lax.axis_size("tp")
    experts = lax.axis_size("ep")
    top = expert_ids.shape[1]
    capacity = max(2, (3 * tok_rows * top + 2 * experts - 1) // (2 * experts))
    flat = expert_ids.reshape(-1)
    onehot = (flat[:, None] == jnp.arange(experts, dtype=jnp.int32)[None, :]).astype(jnp.int32)
    earlier = jnp.cumsum(onehot, axis=0) - onehot
    slot = jnp.sum(earlier * onehot, axis=-1)
    position = flat * capacity + slot
    owner = jnp.arange(flat.shape[0], dtype=jnp.int32) // top
    w_gate = gate_weight[0]
    w_up = up_weight[0]
    w_down = down_weight[0]
    send = jnp.zeros((experts * capacity, half), jnp.bfloat16).at[position].set(tokens[owner])
    send = send.reshape(experts, capacity, half)
    received = lax.all_to_all(send, "ep", split_axis=0, concat_axis=0, tiled=True)
    sources = received.shape[0]
    count = received.shape[1]
    whole_rows = lax.all_gather(received, "tp", axis=2, tiled=True)
    rows = normalize(whole_rows.reshape(sources * count, width), norm_gain)
    gate = jnp.dot(rows, w_gate, preferred_element_type=jnp.float32)
    upper = jnp.dot(rows, w_up, preferred_element_type=jnp.float32)
    hidden = (jax.nn.silu(gate) * upper).astype(jnp.bfloat16)
    result = jnp.dot(collect(hidden, "tp", 1), w_down, preferred_element_type=jnp.float32)
    result = result.astype(jnp.bfloat16).reshape(sources, count, half)
    back = cut_exchange(result, "ep", 2, 0, 0)
    picked = back.reshape(experts * capacity, half)[position].astype(jnp.float32)
    picked = picked * route_weights.reshape(-1)[:, None]
    return jnp.sum(picked.reshape(tok_rows, top, half), axis=1).astype(jnp.bfloat16)


def solution(mesh):
    in_specs = (
        P(("grp", "ep"), "tp"),
        P(),
        P(("grp", "ep"), None),
        P(("grp", "ep"), None),
        P("ep", None, "tp"),
        P("ep", None, "tp"),
        P("ep", None, "tp"),
    )
    out_specs = P(("grp", "ep"), "tp")
    return jax.shard_map(
        on_device, mesh=mesh, in_specs=in_specs, out_specs=out_specs, check_vma=False
    )
```

profile of v0, /device:TPU:515, one launch (start us, length us, event | category | flops | bytes accessed | tf_op | source)
XLA Modules:
  0.0 320.1 jit_solution(3808967039707982934)
XLA Ops:
  6.5 0.0 copy-start
  6.6 0.0 all-gather.2.cloned.1.call-start
  6.6 0.9 copy.26
  7.5 0.2 eq.29
  7.6 0.2 eq.25
  7.8 0.7 broadcast_multiply_fusion
  8.5 18.0 %reduce-window.6 = s32[64,8,128]{2,1,0:T(8,128)S(1)} reduce-window(s32[64,8,128]{2,1,0:T(8,128)S(1)} %fusion.14, s32[]{:T(128)} %constant.31.clone.1), window={size=1x1x128 pad=0_0x0_0x127_0}, to_apply=%region_0.0 | reduce-window | flops 8323072 | bytes 524292 | tf_op jit(solution)/shard_map/reduce-window
  26.6 0.1 slice.12
  26.7 0.1 copy.28
  26.9 0.1 copy.29
  27.0 0.1 broadcast_add_fusion
  27.1 0.1 copy.25
  27.3 0.2 mul.61
  27.5 0.1 fusion.13
  27.5 0.0 copy-done
  27.6 14.8 %scatter_custom_fusion = bf16[1536,1024]{1,0:T(8,128)(2,1)} fusion(s32[1024]{0:T(1024)S(1)} %bitcast.53, bf16[512,1024]{1,0:T(8,128)(2,1)S(1)} %copy-done, s32[1024]{0:T(1024)S(1)} %broadcast_clamp_fusion.1, bf16[]{:T(256)} %constant.29.clone.1), kind=kCustom, calls=%fused_computation.13 | custom fusion | bytes 3145730 | tf_op jit(solution)/shard_map/scatter | solution.py:67
  42.3 87.9 %all_to_all.20 = bf16[64,24,1024]{2,1,0:T(8,128)(2,1)} all-to-all(bf16[64,24,1024]{2,1,0:T(8,128)(2,1)} %bitcast.44), channel_id=1, replica_groups=mesh['grp'=2,'ep'=64,'tp'=2] {'ep'}, dimensions={0} | all-to-all | bytes 6291456 | tf_op jit(solution)/shard_map/all_to_all | solution.py:69
  130.2 0.1 all-gather.2.cloned.1.call-update
  130.3 0.0 copy-start.4
  130.3 39.7 %all-gather.2.cloned.1.call-done = bf16[64,24,2048]{2,1,0:T(8,128)(2,1)} async-done(((bf16[64,24,1024]{2,1,0:T(8,128)(2,1)}), bf16[64,24,2048]{2,1,0:T(8,128)(2,1)}) %all-gather.2.cloned.1.call-update) | async-done | bytes 6291472 | tf_op jit(solution)/shard_map/all_gather | solution.py:72
  170.1 4.2 %fusion = f32[64,24]{1,0:T(8,128)S(1)} fusion(bf16[64,24,2048]{2,1,0:T(8,128)(2,1)} %all-gather.2.cloned.1.call-done), kind=kLoop, calls=%fused_computation.5 | loop fusion | flops 9435648 | bytes 6297600 | tf_op jit(solution)/shard_map/reduce_sum | solution.py:48
  174.3 0.0 copy-done.4
  174.3 0.3 copy-done.1
  174.7 1.5 fusion.2
  176.2 0.0 copy-done.6
  176.2 0.0 copy-start.7
  176.2 1.9 fusion.9
  178.1 0.0 copy-done.7
  178.1 2.1 fusion.3
  180.1 0.3 copy.30
  180.4 0.0 copy-start.8
  180.4 0.1 broadcast_in_dim.5
  180.6 5.0 %all_to_all.21 = bf16[2,1536,256]{1,2,0:T(8,128)(2,1)S(1)} all-to-all(bf16[2,1536,256]{1,2,0:T(8,128)(2,1)S(1)} %broadcast_in_dim.5), channel_id=1, replica_groups=mesh['grp'=2,'ep'=64,'tp'=2] {'tp'}, dimensions={0} | all-to-all | bytes 3145728 | tf_op jit(solution)/shard_map/all_to_all | solution.py:9
  185.5 0.0 copy-done.8
  185.6 1.8 convolution_convert_fusion
  187.4 1.7 copy-done.3
  189.1 1.0 split.8
  190.1 13.1 %all-to-all-start.2 = ((bf16[64,1,8,1024]{3,2,1,0:T(8,128)(2,1)}), bf16[64,1,8,1024]{3,2,1,0:T(8,128)(2,1)S(1)}, u32[]{:S(2)}, u32[]{:S(2)}) async-start(bf16[64,1,8,1024]{3,2,1,0:T(8,128)(2,1)} %split.8), calls=%async_computation.2 | async-start | bytes 2097152 | tf_op jit(solution)/shard_map/all_to_all | solution.py:42
  203.2 3.3 %split.9 = bf16[64,1,16,1024]{3,2,1,0:T(8,128)(2,1)} slice(bf16[64,1,24,1024]{3,2,1,0:T(8,128)(2,1)} %bitcast.48), slice={[0:64], [0:1], [8:24], [0:1024]} | slice | bytes 4194304 | tf_op jit(solution)/shard_map/split | solution.py:40
  206.5 24.4 %all-to-all-done.2 = bf16[64,1,8,1024]{3,2,1,0:T(8,128)(2,1)S(1)} async-done(((bf16[64,1,8,1024]{3,2,1,0:T(8,128)(2,1)}), bf16[64,1,8,1024]{3,2,1,0:T(8,128)(2,1)S(1)}, u32[]{:S(2)}, u32[]{:S(2)}) %all-to-all-start.2) | async-done | bytes 1048608 | tf_op jit(solution)/shard_map/all_to_all | solution.py:42
  231.0 1.0 copy-done.2
  232.0 8.1 %all-to-all-start.3 = ((bf16[64,1,16,1024]{3,2,1,0:T(8,128)(2,1)}), bf16[64,1,16,1024]{3,2,1,0:T(8,128)(2,1)S(1)}, u32[]{:S(2)}, u32[]{:S(2)}) async-start(bf16[64,1,16,1024]{3,2,1,0:T(8,128)(2,1)} %split.9), calls=%async_computation.3 | async-start | bytes 4194304 | tf_op jit(solution)/shard_map/all_to_all | solution.py:42
  240.1 0.1 copy.33
  240.2 49.8 %all-to-all-done.3 = bf16[64,1,16,1024]{3,2,1,0:T(8,128)(2,1)S(1)} async-done(((bf16[64,1,16,1024]{3,2,1,0:T(8,128)(2,1)}), bf16[64,1,16,1024]{3,2,1,0:T(8,128)(2,1)S(1)}, u32[]{:S(2)}, u32[]{:S(2)}) %all-to-all-start.3) | async-done | bytes 2097184 | tf_op jit(solution)/shard_map/all_to_all | solution.py:42
  290.1 3.3 %pad_maximum_fusion = bf16[64,1,24,1024]{3,2,1,0:T(8,128)(2,1)} fusion(bf16[64,1,16,1024]{3,2,1,0:T(8,128)(2,1)S(1)} %all-to-all-done.3, bf16[64,1,8,1024]{3,2,1,0:T(8,128)(2,1)} %copy-done.2), kind=kLoop, calls=%fused_computation.10 | loop fusion | flops 6291456 | bytes 6291456 | tf_op jit(solution)/shard_map/concatenate | solution.py:43
  293.4 7.3 %gather_fusion = bf16[1024,1024]{1,0:T(8,128)(2,1)S(1)} fusion(bf16[1536,1024]{1,0:T(8,128)(2,1)} %bitcast.43, s32[1024]{0:T(1024)S(1)} %broadcast_clamp_fusion), kind=kCustom, calls=%fused_computation.1 | custom fusion | bytes 4198400 | tf_op jit(solution)/shard_map/gather | solution.py:80
  300.7 4.0 %reshape.142 = f32[512,2,1024]{2,1,0:T(2,128)} reshape(bf16[1024,1024]{1,0:T(8,128)(2,1)S(1)} %gather_fusion) | data formatting | bytes 6291456 | tf_op jit(solution)/shard_map/convert_element_type | solution.py:80
  304.7 8.6 %multiply_reduce_fusion = bf16[512,1024]{1,0:T(8,128)(2,1)} fusion(f32[512,2,1024]{2,1,0:T(2,128)} %reshape.142, f32[512,2]{1,0:T(8,128)S(1)} %copy.33), kind=kLoop, calls=%fused_computation.8 | loop fusion | flops 1572864 | bytes 5246976 | tf_op jit(solution)/shard_map/reduce_sum | solution.py:82
  (14 shorter events, 0.1 us)
Async XLA Ops:
  6.5 21.0 %copy-start = (bf16[512,1024]{1,0:T(8,128)(2,1)S(1)}, bf16[512,1024]{1,0:T(8,128)(2,1)}, u32[]{:S(2)}) copy-start(bf16[512,1024]{1,0:T(8,128)(2,1)} %param.7) | copy-start | bytes 3145732
  6.6 163.5 %all-gather.2.cloned.1.call-start = ((), (), s32[]{:S(2)}) async-start(), calls=%async_computation.4 | async-start | bytes 9437184 | tf_op jit(solution)/shard_map/all_gather | solution.py:72
  130.3 44.0 %copy-start.4 = (f32[2048]{0:T(1024)S(1)}, f32[2048]{0:T(1024)}, u32[]{:S(2)}) copy-start(f32[2048]{0:T(1024)} %param.8) | copy-start | bytes 24580
  170.1 4.6 %copy-start.1 = (bf16[64,24,2048]{2,1,0:T(8,128)(2,1)S(1)}, bf16[64,24,2048]{2,1,0:T(8,128)(2,1)}, u32[]{:S(2)}) copy-start(bf16[64,24,2048]{2,1,0:T(8,128)(2,1)} %all-gather.2.cloned.1.call-done) | copy-start | bytes 18874372
  174.7 1.5 copy-start.6
  176.2 1.9 copy-start.7
  180.4 5.1 %copy-start.8 = (bf16[1,512,1024]{2,1,0:T(8,128)(2,1)S(1)}, bf16[1,512,1024]{2,1,0:T(8,128)(2,1)}, u32[]{:S(2)}) copy-start(bf16[1,512,1024]{2,1,0:T(8,128)(2,1)} %param.13) | copy-start | bytes 3145732
  187.4 1.7 copy-start.3
  190.1 40.9 %all-to-all-start.2 = ((bf16[64,1,8,1024]{3,2,1,0:T(8,128)(2,1)}), bf16[64,1,8,1024]{3,2,1,0:T(8,128)(2,1)S(1)}, u32[]{:S(2)}, u32[]{:S(2)}) async-start(bf16[64,1,8,1024]{3,2,1,0:T(8,128)(2,1)} %split.8), calls=%async_computation.2 | async-start | bytes 2097152 | tf_op jit(solution)/shard_map/all_to_all | solution.py:42
  206.5 33.5 %copy-start.5 = (f32[512,2]{0,1:T(2,128)S(1)}, f32[512,2]{0,1:T(2,128)}, u32[]{:S(2)}) copy-start(f32[512,2]{0,1:T(2,128)} %param.10) | copy-start | bytes 12292
  231.0 1.0 copy-start.2
  232.0 58.1 %all-to-all-start.3 = ((bf16[64,1,16,1024]{3,2,1,0:T(8,128)(2,1)}), bf16[64,1,16,1024]{3,2,1,0:T(8,128)(2,1)S(1)}, u32[]{:S(2)}, u32[]{:S(2)}) async-start(bf16[64,1,16,1024]{3,2,1,0:T(8,128)(2,1)} %split.9), calls=%async_computation.3 | async-start | bytes 4194304 | tf_op jit(solution)/shard_map/all_to_all | solution.py:42
Sparse Core Ops, SparseCore 0:
  130.4 39.5 all-gather.1
where the time goes:
time: 323 us; the launch traced here: 320 us
  waiting for transfers between devices  114 us (35%)
  blocking collectives  92.9 us (29%)
  other arithmetic  36.6 us (11%)
  local copies, waits for them, and re-layouts  35.8 us (11%)
  starting transfers between devices  21.2 us (7%)
  between operations  13.7 us (4%)
  matrix products  5.78 us (2%)
    all_to_all x1, blocking collectives, on_device(): lax.all_to_all(send, 'ep', split_axis=0, concat_axis=0, tiled=True)  87.9 us
    all_to_all x2, waiting for transfers between devices, cut_exchange(): lax.all_to_all(section, axis, split_axis=0, concat_axis=0, tiled=True)  74.3 us
    all_gather x1, waiting for transfers between devices, on_device(): whole_rows = lax.all_gather(received, 'tp', axis=2, tiled=True)  39.7 us
    all_to_all x2, starting transfers between devices, cut_exchange(): lax.all_to_all(section, axis, split_axis=0, concat_axis=0, tiled=True)  21.2 us
    another operation x3, other arithmetic  18.2 us
    scatter x1, local copies, waits for them, and re-layouts, on_device(): jnp.zeros((experts * capacity, half), jnp.bfloat16).at[position]  14.8 us
    reduce_sum x1, other arithmetic, on_device(): jnp.sum(picked.reshape(tok_rows, top, half), axis=1).astype(jnp.bfloat16)  8.58 us
    gather x1, local copies, waits for them, and re-layouts, on_device(): back.reshape(experts * capacity, half)[position].astype(jnp.float32)  7.27 us
  transfers between devices with their start and end apart: 3, of which 3 were waited for; matrix products, arithmetic and copies ran while one was open for 1% of the time, Pallas kernels for 0%

commit v1 on v0

v1 whole, which is shorter than its diff:
```python
import functools
import math

import jax
import jax.numpy as jnp
from jax import lax
from jax.experimental import pallas as pl
from jax.experimental.pallas import tpu as pltpu
from jax.sharding import PartitionSpec as P

MESH = pl.DeviceIdType.MESH
BF16 = jnp.bfloat16
F32 = jnp.float32


def wrapped(v, side):
    v = jnp.where(v < 0, v + side, v)
    return jnp.where(v >= side, v - side, v)


def kernel(
    side, cap,
    tok, gain, ids, wts, gate_hbm, up_hbm, down_hbm, out,
    wg, wu, wd, snd, rl1, rcv, res, rl2, back, normed, acc, posr, wts_hi_lo,
    s_w, r_w, l_w, s_a, s_b, s_c, s_d, r1, r2, r3, r4,
):
    S = side
    c = lax.axis_index("tp")
    ep = lax.axis_index("ep")
    y = ep // S
    x = ep % S
    s = 1 - 2 * c
    tok_rows = tok.shape[0]
    half = tok.shape[1]
    blocks = cap // 8

    def at(dx, dy):
        return ((y + dy + S) % S) * S + (x + dx + S) % S

    def send(src, dst, send_sem, recv_sem, chip, core):
        pltpu.make_async_remote_copy(
            src_ref=src, dst_ref=dst, send_sem=send_sem, recv_sem=recv_sem,
            device_id={"ep": chip, "tp": core}, device_id_type=MESH,
        ).start()

    def wait(sem, ref):
        pltpu.make_async_copy(ref, ref, sem).wait()

    barrier = pltpu.get_barrier_semaphore()
    for d in range(1, S):
        for h in range(2):
            pl.semaphore_signal(barrier, inc=1, device_id={"ep": at(d, 0), "tp": h}, device_id_type=MESH)
            pl.semaphore_signal(barrier, inc=1, device_id={"ep": at(0, d), "tp": h}, device_id_type=MESH)
    pl.semaphore_signal(barrier, inc=1, device_id={"ep": ep, "tp": 1 - c}, device_id_type=MESH)

    weights = ((gate_hbm, wg), (up_hbm, wu), (down_hbm, wd))
    for i, (src, dst) in enumerate(weights):
        pltpu.make_async_copy(src.at[0], dst.at[c], l_w.at[i]).start()

    row = lax.broadcasted_iota(jnp.int32, (128, tok_rows), 0)
    e0 = ids[0:1, :]
    e1 = ids[1:2, :]
    hot0 = (row == e0).astype(F32)
    hot1 = (row == e1).astype(F32)
    earlier = (
        lax.broadcasted_iota(jnp.int32, (tok_rows, tok_rows), 0)
        < lax.broadcasted_iota(jnp.int32, (tok_rows, tok_rows), 1)
    )
    rank = jnp.dot(
        (hot0 + hot1).astype(BF16), earlier.astype(F32).astype(BF16), preferred_element_type=F32
    )
    pos0 = jnp.sum(rank * hot0, axis=0, keepdims=True) + (e0 * cap).astype(F32)
    pos1 = jnp.sum(rank * hot1, axis=0, keepdims=True) + (e1 * cap).astype(F32)
    w0 = wts[0:1, :]
    w1 = wts[1:2, :]
    w0_hi = w0.astype(BF16).astype(F32)
    w1_hi = w1.astype(BF16).astype(F32)
    row = lax.broadcasted_iota(jnp.int32, (8, tok_rows), 0)
    table = jnp.zeros((8, tok_rows), F32)
    for i, values in enumerate((pos0, pos1, w0_hi, w1_hi, w0 - w0_hi, w1 - w1_hi)):
        table = jnp.where(row == i, values, table)
    posr[...] = table
    table = jnp.concatenate([table, jnp.zeros((120, tok_rows), F32)], axis=0)
    wts_hi_lo[...] = jnp.transpose(table)

    def coords(j, k):
        t = (j + s * k + S) % S
        return t, j * (1 - c) + t * c, j * c + t * (1 - c)

    def positions(k, shape, dim):
        i = lax.broadcasted_iota(jnp.int32, shape, dim)
        j = jnp.zeros(shape, jnp.int32)
        for m in range(1, S):
            j = j + (i >= m * cap).astype(jnp.int32)
        t = wrapped(j + s * k, S)
        dx = jnp.where(c == 0, j, t)
        dy = jnp.where(c == 0, t, j)
        e = wrapped(y + dy, S) * S + wrapped(x + dx, S)
        return (e * cap + i - j * cap).astype(F32)

    def gather(k):
        p = positions(k, (S * cap, 1), 0)
        pick = jnp.where(p == posr[0:1, :], 1.0, jnp.where(p == posr[1:2, :], 1.0, 0.0))
        rows = jnp.dot(pick.astype(BF16), tok[...], preferred_element_type=F32)
        snd[k] = rows.reshape(S, blocks, 8, half).astype(BF16)

    def dispatch(k):
        for j in range(S):
            t, dx, dy = coords(j, k)
            p = dx % 2
            q = dx // 2
            if j == 0:
                @pl.when(t != 0)
                def _():
                    send(snd.at[k, j], rcv.at[k, q, c], s_a.at[k, j], r2.at[k, q, c], at(dx, dy), p)

                @pl.when((t == 0) & (c == 1))
                def _():
                    send(snd.at[k, j], rcv.at[k, q, c], s_a.at[k, j], r2.at[k, q, c], ep, 0)

                @pl.when((t == 0) & (c == 0))
                def _():
                    rcv[0, 0, 0] = snd[0, 0]
            else:
                @pl.when(t != 0)
                def _():
                    send(snd.at[k, j], rl1.at[k, j], s_a.at[k, j], r1.at[k, j], at(j * (1 - c), j * c), c)

                @pl.when(t == 0)
                def _():
                    send(snd.at[k, j], rcv.at[k, q, c], s_a.at[k, j], r2.at[k, q, c], at(dx, dy), p)

    def relay_dispatch(k):
        for j in range(1, S):
            t, dx, dy = coords(j, k)
            p = dx % 2
            q = dx // 2

            @pl.when(t != 0)
            def _():
                wait(r1.at[k, j], rl1.at[k, j])
                send(rl1.at[k, j], rcv.at[k, q, c], s_b.at[k, j], r2.at[k, q, c], at(t * c, t * (1 - c)), p)

    def expert(k):
        rows = cap
        for q in range(S // 2):
            for h in range(2):
                if q == 0 and h == 0:
                    @pl.when((k != 0) | (c != 0))
                    def _():
                        wait(r2.at[k, q, h], rcv.at[k, q, h])
                else:
                    wait(r2.at[k, q, h], rcv.at[k, q, h])
        for q in range(S // 2):
            xa = rcv[k, q, 0].astype(F32).reshape(rows, half)
            xb = rcv[k, q, 1].astype(F32).reshape(rows, half)
            squares = jnp.sum(xa * xa, axis=1, keepdims=True) + jnp.sum(xb * xb, axis=1, keepdims=True)
            scale = lax.rsqrt(squares * (1.0 / (2 * half)) + 1e-06)
            normed[q * rows : (q + 1) * rows, :half] = xa * scale * gain[:, :half]
            normed[q * rows : (q + 1) * rows, half:] = xb * scale * gain[:, half:]
        xn = normed[...].astype(BF16)
        hidden = []
        for i in range(2):
            gate = jnp.dot(xn, wg[i], preferred_element_type=F32)
            upper = jnp.dot(xn, wu[i], preferred_element_type=F32)
            hidden.append((gate / (1.0 + jnp.exp(-gate)) * upper).astype(BF16))
        hidden = jnp.concatenate(hidden, axis=1)
        for h in range(2):
            result = jnp.dot(hidden, wd[h], preferred_element_type=F32)
            result = result.reshape(S // 2, blocks, 8, half).astype(BF16)
            for q in range(S // 2):
                res[k, q, h] = result[q]
        for q in range(S // 2):
            dx = 2 * q + c
            dy = (dx + k) % S
            direct = (dx == 0) | (dy == 0)
            for h in range(2):
                j = dy if h else dx

                @pl.when(jnp.logical_not(direct))
                def _():
                    chip = at(0, -dy) if h else at(-dx, 0)
                    send(res.at[k, q, h], rl2.at[k, j], s_c.at[k, q, h], r3.at[k, j], chip, h)

                away = direct if h else direct & ((dx != 0) | (dy != 0))

                @pl.when(away)
                def _():
                    send(res.at[k, q, h], back.at[k, j], s_c.at[k, q, h], r4.at[k, j], at(-dx, -dy), h)

                if q == 0 and h == 0:
                    @pl.when((k == 0) & (c == 0))
                    def _():
                        back[0, 0] = res[0, 0, 0]

    def relay_return(k):
        for j in range(1, S):
            t, dx, dy = coords(j, k)

            @pl.when(t != 0)
            def _():
                wait(r3.at[k, j], rl2.at[k, j])
                send(rl2.at[k, j], back.at[k, j], s_d.at[k, j], r4.at[k, j], at(-t * c, -t * (1 - c)), c)

    def combine(k):
        for j in range(S):
            if j == 0:
                @pl.when((k != 0) | (c != 0))
                def _():
                    wait(r4.at[k, j], back.at[k, j])
            else:
                wait(r4.at[k, j], back.at[k, j])
        p = positions(k, (1, S * cap), 1)
        first = p == wts_hi_lo[:, 0:1]
        second = p == wts_hi_lo[:, 1:2]
        hi = jnp.where(first, wts_hi_lo[:, 2:3], jnp.where(second, wts_hi_lo[:, 3:4], 0.0)).astype(BF16)
        lo = jnp.where(first, wts_hi_lo[:, 4:5], jnp.where(second, wts_hi_lo[:, 5:6], 0.0)).astype(BF16)
        rows = back[k].astype(F32).reshape(S * cap, half).astype(BF16)
        acc[...] += jnp.dot(hi, rows, preferred_element_type=F32) + jnp.dot(lo, rows, preferred_element_type=F32)

    def loop(low, high, *steps):
        def body(k, _):
            for step in steps:
                step(k)
            return 0

        lax.fori_loop(low, high, body, 0)

    gather(0)
    pl.semaphore_wait(barrier, 4 * (S - 1) + 1)
    dispatch(0)
    for i, (src, dst) in enumerate(weights):
        send(src.at[0], dst.at[c], s_w.at[i], r_w.at[i], ep, 1 - c)
    loop(1, S, gather, dispatch)
    acc[...] = jnp.zeros_like(acc)
    ahead = min(2, S)
    loop(0, ahead, relay_dispatch)
    for i, (src, dst) in enumerate(weights):
        wait(l_w.at[i], dst.at[c])
        wait(r_w.at[i], dst.at[1 - c])

    def relay_and_expert(k):
        @pl.when(k + ahead < S)
        def _():
            relay_dispatch(k + ahead)

        expert(k)

    loop(0, S, relay_and_expert)

    def relay_and_combine(k):
        @pl.when(k < S)
        def _():
            relay_return(k)

        @pl.when(k >= ahead)
        def _():
            combine(k - ahead)

    loop(0, S + ahead, relay_and_combine)
    out[...] = acc[...].astype(BF16)

    def sent(k):
        for j in range(S):
            if j == 0:
                @pl.when((k != 0) | (c != 0))
                def _():
                    wait(s_a.at[k, j], snd.at[k, j])
            else:
                wait(s_a.at[k, j], snd.at[k, j])

                @pl.when((j + s * k + S) % S != 0)
                def _():
                    wait(s_b.at[k, j], rl1.at[k, j])
                    wait(s_d.at[k, j], rl2.at[k, j])
        for q in range(S // 2):
            for h in range(2):
                if q == 0 and h == 0:
                    @pl.when((k != 0) | (c != 0))
                    def _():
                        wait(s_c.at[k, q, h], res.at[k, q, h])
                else:
                    wait(s_c.at[k, q, h], res.at[k, q, h])

    loop(0, S, sent)
    for i, (src, dst) in enumerate(weights):
        wait(s_w.at[i], dst.at[c])


def on_device(tokens, norm_gain, expert_ids, route_weights, gate_weight, up_weight, down_weight):
    tok_rows, half = tokens.shape
    experts = lax.axis_size("ep")
    side = math.isqrt(experts)
    top = expert_ids.shape[1]
    cap = max(2, (3 * tok_rows * top + 2 * experts - 1) // (2 * experts))
    width, part = gate_weight.shape[1:]
    S = side
    block = (cap // 8, 8, half)
    vmem = pl.BlockSpec(memory_space=pltpu.VMEM)
    hbm = pl.BlockSpec(memory_space=pl.ANY)
    dma = pltpu.SemaphoreType.DMA
    return pl.pallas_call(
        functools.partial(kernel, side, cap),
        out_shape=jax.ShapeDtypeStruct((tok_rows, half), BF16),
        in_specs=[vmem] * 4 + [hbm] * 3,
        out_specs=vmem,
        scratch_shapes=[
            pltpu.VMEM((2, width, part), BF16),
            pltpu.VMEM((2, width, part), BF16),
            pltpu.VMEM((2, 2 * part, half), BF16),
            pltpu.VMEM((S, S) + block, BF16),
            pltpu.VMEM((S, S) + block, BF16),
            pltpu.VMEM((S, S // 2, 2) + block, BF16),
            pltpu.VMEM((S, S // 2, 2) + block, BF16),
            pltpu.VMEM((S, S) + block, BF16),
            pltpu.VMEM((S, S) + block, BF16),
            pltpu.VMEM((S // 2 * cap, width), F32),
            pltpu.VMEM((tok_rows, half), F32),
            pltpu.VMEM((8, tok_rows), F32),
            pltpu.VMEM((tok_rows, 128), F32),
            dma((3,)), dma((3,)), dma((3,)),
            dma((S, S)), dma((S, S)), dma((S, S // 2, 2)), dma((S, S)),
            dma((S, S)), dma((S, S // 2, 2)), dma((S, S)), dma((S, S)),
        ],
        compiler_params=pltpu.CompilerParams(
            collective_id=0, has_side_effects=True, vmem_limit_bytes=56 * 2**20
        ),
    )(tokens, norm_gain.reshape(1, -1), expert_ids.T, route_weights.T, gate_weight, up_weight, down_weight)


def solution(mesh):
    in_specs = (
        P(("grp", "ep"), "tp"),
        P(),
        P(("grp", "ep"), None),
        P(("grp", "ep"), None),
        P("ep", None, "tp"),
        P("ep", None, "tp"),
        P("ep", None, "tp"),
    )
    out_specs = P(("grp", "ep"), "tp")
    return jax.shard_map(
        on_device, mesh=mesh, in_specs=in_specs, out_specs=out_specs, check_vma=False
    )
```

time: 323 us -> 171 us (0.53)
  Pallas kernels: 0 us -> 169 us
  waiting for transfers between devices: 114 us -> 0 us
  blocking collectives: 92.9 us -> 0 us
  other arithmetic: 36.6 us -> 0 us
  local copies, waits for them, and re-layouts: 35.8 us -> 2.26 us
  starting transfers between devices: 21.2 us -> 0 us
  between operations: 13.7 us -> 0.01 us
  matrix products: 5.78 us -> 0 us
    pallas_call x0 -> x1, Pallas kernels: none -> 169 us  [on_device(): pl.pallas_call(functools.partial(kernel, side, cap), out_shape=jax.ShapeD...]
    all_to_all x2 -> x0, blocking collectives: 92.9 us -> none  [the longest x1 87.9 us: on_device(): lax.all_to_all(send, 'ep', split_axis=0, concat_axis=0, tiled=True)]
    all_to_all x2 -> x0, waiting for transfers between devices: 74.3 us -> none  [cut_exchange(): lax.all_to_all(section, axis, split_axis=0, concat_axis=0, tiled=True)]
    all_gather x1 -> x0, waiting for transfers between devices: 39.7 us -> none  [on_device(): whole_rows = lax.all_gather(received, 'tp', axis=2, tiled=True)]
    all_to_all x2 -> x0, starting transfers between devices: 21.2 us -> none  [cut_exchange(): lax.all_to_all(section, axis, split_axis=0, concat_axis=0, tiled=True)]
    another operation x3 -> x0, other arithmetic: 18.2 us -> none
    scatter x1 -> x0, local copies, waits for them, and re-layouts: 14.8 us -> none  [on_device(): jnp.zeros((experts * capacity, half), jnp.bfloat16).at[position]]
    reduce_sum x3 -> x0, other arithmetic: 12.9 us -> none  [the longest x1 8.58 us: on_device(): jnp.sum(picked.reshape(tok_rows, top, half), axis=1).astype(jnp.bfloat16)]
  transfers between devices with their start and end apart: 3 -> 0, of which waited for: 3 -> 0; matrix products, arithmetic and copies ran while one was open for 1% -> 0% of each run, Pallas kernels for 0% -> 0%
where the time goes in v1:
time: 171 us
  Pallas kernels  169 us (99%)
  local copies, waits for them, and re-layouts  2.26 us (1%)
    pallas_call x1, Pallas kernels, on_device(): pl.pallas_call(functools.partial(kernel, side, cap), out_shape=jax.ShapeD...  169 us

profile of v1, /device:TPU:515, one launch (start us, length us, event | category | flops | bytes accessed | tf_op | source)
XLA Modules:
  0.0 170.9 jit_solution(3708185437490507827)
XLA Ops:
  0.0 168.6 %shard_map.73 = bf16[512,1024]{1,0:T(8,128)(2,1)} custom-call(bf16[512,1024]{1,0:T(8,128)(2,1)} %tok.1, f32[1,2048]{1,0:T(1,128)} %bitcast.3, s32[2,512]{1,0:T(2,128)} %bitcast.4, f32[2,512]{1,0:T(2,128)} %bitcast.5, bf16[1,2048,256]{2,1,0:T(8,128)(2,1)} %gate_hbm.1, bf16[1,2048,256]{2,1,0:T(8,128)(2,1)} %up_hbm.1, bf16[1,512,1024]{2,1,0:T(8,128)(2,1)} %down_hbm.1), custom_call_target="tpu_custom_call" | custom-call | tf_op jit(solution)/shard_map/pallas_call | solution.py:302
  168.6 2.3 %copy.9 = bf16[512,1024]{1,0:T(8,128)(2,1)} copy(bf16[512,1024]{1,0:T(8,128)(2,1)} %shard_map.73) | data formatting | bytes 2097152

commit v2 on v1

v2 whole, which is shorter than its diff:
```python
import functools
import math

import jax
import jax.numpy as jnp
from jax import lax
from jax.experimental import pallas as pl
from jax.experimental.pallas import tpu as pltpu
from jax.sharding import PartitionSpec as P

MESH = pl.DeviceIdType.MESH
BF16 = jnp.bfloat16
F32 = jnp.float32


def wrapped(v, side):
    v = jnp.where(v < 0, v + side, v)
    return jnp.where(v >= side, v - side, v)


def kernel(
    side, cap,
    tok_hbm, gain, ids, wts, gate_hbm, up_hbm, down_hbm, out,
    tok, wg, wu, wd, snd, rl1, rcv, res, rl2, back, normed, acc, posr, wts_hi_lo,
    s_w, r_w, l_w, l_t, s_a, s_b, s_c, s_d, r1, r2, r3, r3_last, r4,
):
    S = side
    half_side = S // 2
    c = lax.axis_index("tp")
    ep = lax.axis_index("ep")
    y = ep // S
    x = ep % S
    s = 1 - 2 * c
    tok_rows = tok.shape[0]
    half = tok.shape[1]
    blocks = cap // 8

    def at(dx, dy):
        return ((y + dy + S) % S) * S + (x + dx + S) % S

    def send(src, dst, send_sem, recv_sem, chip, core):
        pltpu.make_async_remote_copy(
            src_ref=src, dst_ref=dst, send_sem=send_sem, recv_sem=recv_sem,
            device_id={"ep": chip, "tp": core}, device_id_type=MESH,
        ).start()

    def wait(sem, ref):
        pltpu.make_async_copy(ref, ref, sem).wait()

    tok_copy = pltpu.make_async_copy(tok_hbm, tok, l_t)
    tok_copy.start()

    barrier = pltpu.get_barrier_semaphore()
    for d in range(1, S):
        for h in range(2):
            pl.semaphore_signal(barrier, inc=1, device_id={"ep": at(d, 0), "tp": h}, device_id_type=MESH)
            pl.semaphore_signal(barrier, inc=1, device_id={"ep": at(0, d), "tp": h}, device_id_type=MESH)
    pl.semaphore_signal(barrier, inc=1, device_id={"ep": ep, "tp": 1 - c}, device_id_type=MESH)

    weights = ((gate_hbm, wg), (up_hbm, wu), (down_hbm, wd))
    for i, (src, dst) in enumerate(weights):
        pltpu.make_async_copy(src.at[0], dst.at[c], l_w.at[i]).start()

    row = lax.broadcasted_iota(jnp.int32, (128, tok_rows), 0)
    e0 = ids[0:1, :]
    e1 = ids[1:2, :]
    hot0 = (row == e0).astype(F32)
    hot1 = (row == e1).astype(F32)
    earlier = (
        lax.broadcasted_iota(jnp.int32, (tok_rows, tok_rows), 0)
        < lax.broadcasted_iota(jnp.int32, (tok_rows, tok_rows), 1)
    )
    rank = jnp.dot(
        (hot0 + hot1).astype(BF16), earlier.astype(F32).astype(BF16), preferred_element_type=F32
    )
    pos0 = jnp.sum(rank * hot0, axis=0, keepdims=True) + (e0 * cap).astype(F32)
    pos1 = jnp.sum(rank * hot1, axis=0, keepdims=True) + (e1 * cap).astype(F32)
    posr[0:1, :] = pos0
    posr[1:2, :] = pos1

    def weight_table():
        w0 = wts[0:1, :]
        w1 = wts[1:2, :]
        w0_hi = w0.astype(BF16).astype(F32)
        w1_hi = w1.astype(BF16).astype(F32)
        row = lax.broadcasted_iota(jnp.int32, (128, tok_rows), 0)
        table = jnp.zeros((128, tok_rows), F32)
        columns = (posr[0:1, :], posr[1:2, :], w0_hi, w1_hi, w0 - w0_hi, w1 - w1_hi)
        for i, values in enumerate(columns):
            table = jnp.where(row == i, values, table)
        wts_hi_lo[...] = jnp.transpose(table)

    def coords(j, k):
        t = (j + s * k + S) % S
        return t, j * (1 - c) + t * c, j * c + t * (1 - c)

    def positions(k, i, low, count):
        j = jnp.zeros(i.shape, jnp.int32)
        for m in range(1, count):
            j = j + (i >= m * cap).astype(jnp.int32)
        slot = i - j * cap
        j = j + low
        t = wrapped(j + s * k, S)
        dx = jnp.where(c == 0, j, t)
        dy = jnp.where(c == 0, t, j)
        e = wrapped(y + dy, S) * S + wrapped(x + dx, S)
        return (e * cap + slot).astype(F32)

    def gather(k):
        p = positions(k, lax.broadcasted_iota(jnp.int32, (S * cap, 1), 0), 0, S)
        pick = jnp.where(p == posr[0:1, :], 1.0, jnp.where(p == posr[1:2, :], 1.0, 0.0))
        rows = jnp.dot(pick.astype(BF16), tok[...], preferred_element_type=F32)
        snd[k] = rows.reshape(S, blocks, 8, half).astype(BF16)

    def dispatch(k):
        for j in range(S):
            t, dx, dy = coords(j, k)
            p = dx % 2
            q = dx // 2
            if j == 0:
                @pl.when(t != 0)
                def _():
                    send(snd.at[k, j], rcv.at[k, q, c], s_a, r2.at[k], at(dx, dy), p)

                @pl.when((t == 0) & (c == 1))
                def _():
                    send(snd.at[k, j], rcv.at[k, q, c], s_a, r2.at[k], ep, 0)

                @pl.when((t == 0) & (c == 0))
                def _():
                    rcv[0, 0, 0] = snd[0, 0]
            else:
                @pl.when(t != 0)
                def _():
                    send(snd.at[k, j], rl1.at[k, j], s_a, r1.at[k], at(j * (1 - c), j * c), c)

                @pl.when(t == 0)
                def _():
                    send(snd.at[k, j], rcv.at[k, q, c], s_a, r2.at[k], at(dx, dy), p)

    def wait_blocks(sem, ref, count):
        wait(sem, ref.at[pl.ds(0, count)])

    def wait_relayed(sem, ref, k):
        @pl.when(k == 0)
        def _():
            wait_blocks(sem, ref.at[k], S - 1)

        if S > 2:
            @pl.when(k != 0)
            def _():
                wait_blocks(sem, ref.at[k], S - 2)

    def relay_dispatch(k):
        wait_relayed(r1.at[k], rl1, k)
        for j in range(1, S):
            t, dx, dy = coords(j, k)
            p = dx % 2
            q = dx // 2

            @pl.when(t != 0)
            def _():
                send(rl1.at[k, j], rcv.at[k, q, c], s_b, r2.at[k], at(t * c, t * (1 - c)), p)

    def send_relayed(k, j, src, chip, core):
        @pl.when(k == S - 1)
        def _():
            send(src, rl2.at[k, j], s_c, r3_last.at[j], chip, core)

        @pl.when(k != S - 1)
        def _():
            send(src, rl2.at[k, j], s_c, r3.at[k], chip, core)

    def expert(k):
        rows = cap
        own = (k == 0) & (c == 0)

        @pl.when(own)
        def _():
            wait_blocks(r2.at[k], back.at[k], S - 1)

        @pl.when(jnp.logical_not(own))
        def _():
            wait_blocks(r2.at[k], back.at[k], S)

        for q in range(S // 2):
            xa = rcv[k, q, 0].astype(F32).reshape(rows, half)
            xb = rcv[k, q, 1].astype(F32).reshape(rows, half)
            squares = jnp.sum(xa * xa, axis=1, keepdims=True) + jnp.sum(xb * xb, axis=1, keepdims=True)
            scale = lax.rsqrt(squares * (1.0 / (2 * half)) + 1e-06)
            normed[q * rows : (q + 1) * rows, :half] = xa * scale * gain[:, :half]
            normed[q * rows : (q + 1) * rows, half:] = xb * scale * gain[:, half:]
        xn = normed[...].astype(BF16)
        hidden = []
        for i in range(2):
            gate = jnp.dot(xn, wg[i], preferred_element_type=F32)
            upper = jnp.dot(xn, wu[i], preferred_element_type=F32)
            hidden.append((gate / (1.0 + jnp.exp(-gate)) * upper).astype(BF16))
        hidden = jnp.concatenate(hidden, axis=1)
        for h in range(2):
            result = jnp.dot(hidden, wd[h], preferred_element_type=F32)
            result = result.reshape(S // 2, blocks, 8, half).astype(BF16)
            for q in range(S // 2):
                res[k, q, h] = result[q]
        for q in range(S // 2):
            dx = 2 * q + c
            dy = (dx + k) % S
            direct = (dx == 0) | (dy == 0)
            for h in range(2):
                j = dy if h else dx

                @pl.when(jnp.logical_not(direct))
                def _():
                    chip = at(0, -dy) if h else at(-dx, 0)
                    send_relayed(k, j, res.at[k, q, h], chip, h)

                away = direct if h else direct & ((dx != 0) | (dy != 0))

                @pl.when(away)
                def _():
                    send(res.at[k, q, h], back.at[k, j], s_c, r4.at[k, j // half_side], at(-dx, -dy), h)

                if q == 0 and h == 0:
                    @pl.when((k == 0) & (c == 0))
                    def _():
                        back[0, 0] = res[0, 0, 0]

    def relay_return(k):
        @pl.when(k != S - 1)
        def _():
            wait_relayed(r3.at[k], rl2, k)

        for j in range(1, S):
            t, dx, dy = coords(j, k)

            @pl.when(t != 0)
            def _():
                @pl.when(k == S - 1)
                def _():
                    wait(r3_last.at[j], rl2.at[k, j])

                send(rl2.at[k, j], back.at[k, j], s_d, r4.at[k, j // half_side], at(-t * c, -t * (1 - c)), c)

    def combined(k, part):
        if part == 0:
            own = (k == 0) & (c == 0)

            @pl.when(own)
            def _():
                if half_side > 1:
                    wait_blocks(r4.at[k, part], back.at[k], half_side - 1)

            @pl.when(jnp.logical_not(own))
            def _():
                wait_blocks(r4.at[k, part], back.at[k], half_side)
        else:
            wait_blocks(r4.at[k, part], back.at[k], half_side)
        count = half_side * cap
        i = lax.broadcasted_iota(jnp.int32, (1, 2 * count), 1)
        high = i < count
        p = positions(k, jnp.where(high, i, i - count), part * half_side, half_side)
        one = jnp.where(high, wts_hi_lo[:, 2:3], wts_hi_lo[:, 4:5])
        two = jnp.where(high, wts_hi_lo[:, 3:4], wts_hi_lo[:, 5:6])
        mix = jnp.where(p == wts_hi_lo[:, 0:1], one, jnp.where(p == wts_hi_lo[:, 1:2], two, 0.0))
        rows = back[k, part * half_side : (part + 1) * half_side].astype(F32).reshape(count, half)
        rows = jnp.concatenate([rows, rows], axis=0).astype(BF16)
        return jnp.dot(mix.astype(BF16), rows, preferred_element_type=F32)

    def combine(k):
        for part in range(2):
            acc[...] += combined(k, part)

    def loop(low, high, *steps):
        def body(k, _):
            for step in steps:
                step(k)
            return 0

        lax.fori_loop(low, high, body, 0)

    tok_copy.wait()
    gather(0)
    pl.semaphore_wait(barrier, 4 * (S - 1) + 1)
    dispatch(0)
    for i, (src, dst) in enumerate(weights):
        send(src.at[0], dst.at[c], s_w.at[i], r_w.at[i], ep, 1 - c)
    loop(1, S, gather, dispatch)
    weight_table()
    acc[...] = jnp.zeros_like(acc)
    ahead = min(2, S)
    loop(0, ahead, relay_dispatch)
    for i, (src, dst) in enumerate(weights):
        wait(l_w.at[i], dst.at[c])
        wait(r_w.at[i], dst.at[1 - c])

    def relay_and_expert(k):
        @pl.when(k + ahead < S)
        def _():
            relay_dispatch(k + ahead)

        expert(k)

    loop(0, S, relay_and_expert)

    def relay_and_combine(k):
        @pl.when(k < S)
        def _():
            relay_return(k)

        @pl.when(k >= ahead)
        def _():
            combine(k - ahead)

    loop(0, S + ahead - 1, relay_and_combine)
    acc[...] += combined(S - 1, 0)
    out[...] = (acc[...] + combined(S - 1, 1)).astype(BF16)

    blocks_sent = S * S
    relayed = S - 1 + (S - 1) * (S - 2)

    def all_sent(sem, count):
        rows = count // S
        wait(sem, snd.at[pl.ds(0, rows)])
        if count % S:
            wait(sem, snd.at[0, pl.ds(0, count % S)])

    for sem in (s_a, s_c):
        @pl.when(c == 0)
        def _():
            all_sent(sem, blocks_sent - 1)

        @pl.when(c != 0)
        def _():
            all_sent(sem, blocks_sent)
    for sem in (s_b, s_d):
        all_sent(sem, relayed)
    for i, (src, dst) in enumerate(weights):
        wait(s_w.at[i], dst.at[c])


def on_device(tokens, norm_gain, expert_ids, route_weights, gate_weight, up_weight, down_weight):
    tok_rows, half = tokens.shape
    experts = lax.axis_size("ep")
    side = math.isqrt(experts)
    top = expert_ids.shape[1]
    cap = max(2, (3 * tok_rows * top + 2 * experts - 1) // (2 * experts))
    width, part = gate_weight.shape[1:]
    S = side
    block = (cap // 8, 8, half)
    vmem = pl.BlockSpec(memory_space=pltpu.VMEM)
    hbm = pl.BlockSpec(memory_space=pltpu.HBM)
    dma = pltpu.SemaphoreType.DMA
    return pl.pallas_call(
        functools.partial(kernel, side, cap),
        out_shape=jax.ShapeDtypeStruct((tok_rows, half), BF16),
        in_specs=[hbm] + [vmem] * 3 + [hbm] * 3,
        out_specs=vmem,
        scratch_shapes=[
            pltpu.VMEM((tok_rows, half), BF16),
            pltpu.VMEM((2, width, part), BF16),
            pltpu.VMEM((2, width, part), BF16),
            pltpu.VMEM((2, 2 * part, half), BF16),
            pltpu.VMEM((S, S) + block, BF16),
            pltpu.VMEM((S, S) + block, BF16),
            pltpu.VMEM((S, S // 2, 2) + block, BF16),
            pltpu.VMEM((S, S // 2, 2) + block, BF16),
            pltpu.VMEM((S, S) + block, BF16),
            pltpu.VMEM((S, S) + block, BF16),
            pltpu.VMEM((S // 2 * cap, width), F32),
            pltpu.VMEM((tok_rows, half), F32),
            pltpu.VMEM((8, tok_rows), F32),
            pltpu.VMEM((tok_rows, 128), F32),
            dma((3,)), dma((3,)), dma((3,)), dma,
            dma, dma, dma, dma,
            dma((S,)), dma((S,)), dma((S,)), dma((S,)), dma((S, 2)),
        ],
        compiler_params=pltpu.CompilerParams(
            collective_id=0, has_side_effects=True, vmem_limit_bytes=52 * 2**20
        ),
    )(tokens, norm_gain.reshape(1, -1), expert_ids.T, route_weights.T, gate_weight, up_weight, down_weight)


def solution(mesh):
    in_specs = (
        P(("grp", "ep"), "tp"),
        P(),
        P(("grp", "ep"), None),
        P(("grp", "ep"), None),
        P("ep", None, "tp"),
        P("ep", None, "tp"),
        P("ep", None, "tp"),
    )
    out_specs = P(("grp", "ep"), "tp")
    return jax.shard_map(
        on_device, mesh=mesh, in_specs=in_specs, out_specs=out_specs, check_vma=False
    )
```

time: 171 us -> 165 us (0.965)
  Pallas kernels: 169 us -> 161 us
    pallas_call x1, Pallas kernels: 169 us -> 161 us  [on_device(): pl.pallas_call(functools.partial(kernel, side, cap), out_shape=jax.ShapeD...]
where the time goes in v2:
time: 165 us; the launch traced here: 164 us
  Pallas kernels  161 us (98%)
  local copies, waits for them, and re-layouts  3.04 us (2%)
    pallas_call x1, Pallas kernels, on_device(): pl.pallas_call(functools.partial(kernel, side, cap), out_shape=jax.ShapeD...  161 us

profile of v2, /device:TPU:515, one launch (start us, length us, event | category | flops | bytes accessed | tf_op | source)
XLA Modules:
  0.0 164.2 jit_solution(7494179733163636807)
XLA Ops:
  0.0 0.0 copy-start.1
  0.0 0.7 copy-done.1
  0.7 0.0 copy-start
  0.7 0.7 copy-done
  1.4 0.0 copy-start.2
  1.4 0.7 copy-done.2
  2.1 161.2 %shard_map.73 = bf16[512,1024]{1,0:T(8,128)(2,1)S(1)} custom-call(bf16[512,1024]{1,0:T(8,128)(2,1)} %tok_hbm.1, f32[1,2048]{1,0:T(1,128)S(1)} %bitcast.3, s32[2,512]{1,0:T(2,128)S(1)} %bitcast.4, f32[2,512]{1,0:T(2,128)S(1)} %bitcast.5, bf16[1,2048,256]{2,1,0:T(8,128)(2,1)} %gate_hbm.1, bf16[1,2048,256]{2,1,0:T(8,128)(2,1)} %up_hbm.1, ...), custom_call_target="tpu_custom_call" | custom-call | tf_op jit(solution)/shard_map/pallas_call | solution.py:353
  163.3 1.0 copy.9
Async XLA Ops:
  0.0 0.7 copy-start.1
  0.7 0.7 copy-start
  1.4 0.7 copy-start.2

commit v3 on v2

--- a/solution.py
+++ b/solution.py
@@ -22,7 +22,7 @@
     side, cap,
     tok_hbm, gain, ids, wts, gate_hbm, up_hbm, down_hbm, out,
     tok, wg, wu, wd, snd, rl1, rcv, res, rl2, back, normed, acc, posr, wts_hi_lo,
-    s_w, r_w, l_w, l_t, s_a, s_b, s_c, s_d, r1, r2, r3, r3_last, r4,
+    s_w, r_w, l_w, l_t, go, s_a, s_b, s_c, s_d, r1, r2, r3, r3_last, r4,
 ):
     S = side
     half_side = S // 2
@@ -52,9 +52,8 @@
 
     barrier = pltpu.get_barrier_semaphore()
     for d in range(1, S):
-        for h in range(2):
-            pl.semaphore_signal(barrier, inc=1, device_id={"ep": at(d, 0), "tp": h}, device_id_type=MESH)
-            pl.semaphore_signal(barrier, inc=1, device_id={"ep": at(0, d), "tp": h}, device_id_type=MESH)
+        pl.semaphore_signal(barrier, inc=1, device_id={"ep": at(d, 0), "tp": c}, device_id_type=MESH)
+        pl.semaphore_signal(barrier, inc=1, device_id={"ep": at(0, d), "tp": c}, device_id_type=MESH)
     pl.semaphore_signal(barrier, inc=1, device_id={"ep": ep, "tp": 1 - c}, device_id_type=MESH)
 
     weights = ((gate_hbm, wg), (up_hbm, wu), (down_hbm, wd))
@@ -112,31 +111,40 @@
         rows = jnp.dot(pick.astype(BF16), tok[...], preferred_element_type=F32)
         snd[k] = rows.reshape(S, blocks, 8, half).astype(BF16)
 
-    def dispatch(k):
+    def dispatch(k, crossing):
         for j in range(S):
             t, dx, dy = coords(j, k)
             p = dx % 2
             q = dx // 2
+            now = (p != c) if crossing else (p == c)
             if j == 0:
-                @pl.when(t != 0)
+                @pl.when(now & (t != 0))
                 def _():
                     send(snd.at[k, j], rcv.at[k, q, c], s_a, r2.at[k], at(dx, dy), p)
 
-                @pl.when((t == 0) & (c == 1))
-                def _():
-                    send(snd.at[k, j], rcv.at[k, q, c], s_a, r2.at[k], ep, 0)
-
-                @pl.when((t == 0) & (c == 0))
-                def _():
-                    rcv[0, 0, 0] = snd[0, 0]
+                if not crossing:
+                    @pl.when((t == 0) & (c == 1))
+                    def _():
+                        send(snd.at[k, j], rcv.at[k, q, c], s_a, r2.at[k], ep, 0)
+
+                    @pl.when((t == 0) & (c == 0))
+                    def _():
+                        rcv[0, 0, 0] = snd[0, 0]
             else:
-                @pl.when(t != 0)
-                def _():
-                    send(snd.at[k, j], rl1.at[k, j], s_a, r1.at[k], at(j * (1 - c), j * c), c)
-
-                @pl.when(t == 0)
+                if not crossing:
+                    @pl.when(t != 0)
+                    def _():
+                        send(snd.at[k, j], rl1.at[k, j], s_a, r1.at[k], at(j * (1 - c), j * c), c)
+
+                @pl.when(now & (t == 0))
                 def _():
                     send(snd.at[k, j], rcv.at[k, q, c], s_a, r2.at[k], at(dx, dy), p)
+
+    def dispatch_same(k):
+        dispatch(k, False)
+
+    def dispatch_crossing(k):
+        dispatch(k, True)
 
     def wait_blocks(sem, ref, count):
         wait(sem, ref.at[pl.ds(0, count)])
@@ -280,11 +288,14 @@
 
     tok_copy.wait()
     gather(0)
-    pl.semaphore_wait(barrier, 4 * (S - 1) + 1)
-    dispatch(0)
+    pl.semaphore_wait(barrier, 2 * (S - 1) + 1)
+    pl.semaphore_signal(go, inc=1, device_id={"ep": ep, "tp": 1 - c}, device_id_type=MESH)
+    dispatch_same(0)
     for i, (src, dst) in enumerate(weights):
         send(src.at[0], dst.at[c], s_w.at[i], r_w.at[i], ep, 1 - c)
-    loop(1, S, gather, dispatch)
+    loop(1, S, gather, dispatch_same)
+    pl.semaphore_wait(go, 1)
+    loop(0, S, dispatch_crossing)
     weight_table()
     acc[...] = jnp.zeros_like(acc)
     ahead = min(2, S)
@@ -370,7 +381,7 @@
             pltpu.VMEM((tok_rows, half), F32),
             pltpu.VMEM((8, tok_rows), F32),
             pltpu.VMEM((tok_rows, 128), F32),
-            dma((3,)), dma((3,)), dma((3,)), dma,
+            dma((3,)), dma((3,)), dma((3,)), dma, pltpu.SemaphoreType.REGULAR,
             dma, dma, dma, dma,
             dma((S,)), dma((S,)), dma((S,)), dma((S,)), dma((S, 2)),
         ],

time: 165 us -> 163 us (0.988)
  no operation moved by 1% of the time
where the time goes in v3:
time: 163 us
  Pallas kernels  160 us (98%)
  local copies, waits for them, and re-layouts  3.04 us (2%)
    pallas_call x1, Pallas kernels, on_device(): pl.pallas_call(functools.partial(kernel, side, cap), out_shape=jax.ShapeD...  160 us

profile of v3, /device:TPU:515, one launch (start us, length us, event | category | flops | bytes accessed | tf_op | source)
XLA Modules:
  0.0 162.9 jit_solution(16314282729120579391)
XLA Ops:
  0.0 0.0 copy-start.1
  0.0 0.7 copy-done.1
  0.7 0.0 copy-start
  0.7 0.7 copy-done
  1.4 0.0 copy-start.2
  1.4 0.7 copy-done.2
  2.1 159.9 %shard_map.73 = bf16[512,1024]{1,0:T(8,128)(2,1)S(1)} custom-call(bf16[512,1024]{1,0:T(8,128)(2,1)} %tok_hbm.1, f32[1,2048]{1,0:T(1,128)S(1)} %bitcast.3, s32[2,512]{1,0:T(2,128)S(1)} %bitcast.4, f32[2,512]{1,0:T(2,128)S(1)} %bitcast.5, bf16[1,2048,256]{2,1,0:T(8,128)(2,1)} %gate_hbm.1, bf16[1,2048,256]{2,1,0:T(8,128)(2,1)} %up_hbm.1, ...), custom_call_target="tpu_custom_call" | custom-call | tf_op jit(solution)/shard_map/pallas_call | solution.py:364
  162.0 1.0 copy.9
Async XLA Ops:
  0.0 0.7 copy-start.1
  0.7 0.7 copy-start
  1.4 0.7 copy-start.2

commit v4 on v3

--- a/solution.py
+++ b/solution.py
@@ -30,7 +30,6 @@
     ep = lax.axis_index("ep")
     y = ep // S
     x = ep % S
-    s = 1 - 2 * c
     tok_rows = tok.shape[0]
     half = tok.shape[1]
     blocks = cap // 8
@@ -57,9 +56,6 @@
     pl.semaphore_signal(barrier, inc=1, device_id={"ep": ep, "tp": 1 - c}, device_id_type=MESH)
 
     weights = ((gate_hbm, wg), (up_hbm, wu), (down_hbm, wd))
-    for i, (src, dst) in enumerate(weights):
-        pltpu.make_async_copy(src.at[0], dst.at[c], l_w.at[i]).start()
-
     row = lax.broadcasted_iota(jnp.int32, (128, tok_rows), 0)
     e0 = ids[0:1, :]
     e1 = ids[1:2, :]
@@ -89,9 +85,13 @@
             table = jnp.where(row == i, values, table)
         wts_hi_lo[...] = jnp.transpose(table)
 
+    def first_axis(core, k):
+        return (core + k) % 2
+
     def coords(j, k):
-        t = (j + s * k + S) % S
-        return t, j * (1 - c) + t * c, j * c + t * (1 - c)
+        f = first_axis(c, k)
+        t = (j + (1 - 2 * f) * k + S) % S
+        return t, j * (1 - f) + t * f, j * f + t * (1 - f)
 
     def positions(k, i, low, count):
         j = jnp.zeros(i.shape, jnp.int32)
@@ -99,9 +99,10 @@
             j = j + (i >= m * cap).astype(jnp.int32)
         slot = i - j * cap
         j = j + low
-        t = wrapped(j + s * k, S)
-        dx = jnp.where(c == 0, j, t)
-        dy = jnp.where(c == 0, t, j)
+        f = first_axis(c, k)
+        t = wrapped(j + (1 - 2 * f) * k, S)
+        dx = jnp.where(f == 0, j, t)
+        dy = jnp.where(f == 0, t, j)
         e = wrapped(y + dy, S) * S + wrapped(x + dx, S)
         return (e * cap + slot).astype(F32)
 
@@ -112,6 +113,7 @@
         snd[k] = rows.reshape(S, blocks, 8, half).astype(BF16)
 
     def dispatch(k, crossing):
+        f = first_axis(c, k)
         for j in range(S):
             t, dx, dy = coords(j, k)
             p = dx % 2
@@ -134,7 +136,7 @@
                 if not crossing:
                     @pl.when(t != 0)
                     def _():
-                        send(snd.at[k, j], rl1.at[k, j], s_a, r1.at[k], at(j * (1 - c), j * c), c)
+                        send(snd.at[k, j], rl1.at[k, j], s_a, r1.at[k], at(j * (1 - f), j * f), c)
 
                 @pl.when(now & (t == 0))
                 def _():
@@ -161,6 +163,7 @@
 
     def relay_dispatch(k):
         wait_relayed(r1.at[k], rl1, k)
+        f = first_axis(c, k)
         for j in range(1, S):
             t, dx, dy = coords(j, k)
             p = dx % 2
@@ -168,7 +171,7 @@
 
             @pl.when(t != 0)
             def _():
-                send(rl1.at[k, j], rcv.at[k, q, c], s_b, r2.at[k], at(t * c, t * (1 - c)), p)
+                send(rl1.at[k, j], rcv.at[k, q, c], s_b, r2.at[k], at(t * f, t * (1 - f)), p)
 
     def send_relayed(k, j, src, chip, core):
         @pl.when(k == S - 1)
@@ -215,12 +218,12 @@
             dy = (dx + k) % S
             direct = (dx == 0) | (dy == 0)
             for h in range(2):
-                j = dy if h else dx
+                f = first_axis(h, k)
+                j = dx * (1 - f) + dy * f
 
                 @pl.when(jnp.logical_not(direct))
                 def _():
-                    chip = at(0, -dy) if h else at(-dx, 0)
-                    send_relayed(k, j, res.at[k, q, h], chip, h)
+                    send_relayed(k, j, res.at[k, q, h], at(-dx * (1 - f), -dy * f), h)
 
                 away = direct if h else direct & ((dx != 0) | (dy != 0))
 
@@ -234,6 +237,8 @@
                         back[0, 0] = res[0, 0, 0]
 
     def relay_return(k):
+        f = first_axis(c, k)
+
         @pl.when(k != S - 1)
         def _():
             wait_relayed(r3.at[k], rl2, k)
@@ -247,7 +252,7 @@
                 def _():
                     wait(r3_last.at[j], rl2.at[k, j])
 
-                send(rl2.at[k, j], back.at[k, j], s_d, r4.at[k, j // half_side], at(-t * c, -t * (1 - c)), c)
+                send(rl2.at[k, j], back.at[k, j], s_d, r4.at[k, j // half_side], at(-t * f, -t * (1 - f)), c)
 
     def combined(k, part):
         if part == 0:
@@ -291,14 +296,15 @@
     pl.semaphore_wait(barrier, 2 * (S - 1) + 1)
     pl.semaphore_signal(go, inc=1, device_id={"ep": ep, "tp": 1 - c}, device_id_type=MESH)
     dispatch_same(0)
+    loop(1, S, gather, dispatch_same)
     for i, (src, dst) in enumerate(weights):
         send(src.at[0], dst.at[c], s_w.at[i], r_w.at[i], ep, 1 - c)
-    loop(1, S, gather, dispatch_same)
+        pltpu.make_async_copy(src.at[0], dst.at[c], l_w.at[i]).start()
     pl.semaphore_wait(go, 1)
     loop(0, S, dispatch_crossing)
     weight_table()
     acc[...] = jnp.zeros_like(acc)
-    ahead = min(2, S)
+    ahead = min(3, S)
     loop(0, ahead, relay_dispatch)
     for i, (src, dst) in enumerate(weights):
         wait(l_w.at[i], dst.at[c])

time: 163 us -> 162 us (level); the launches traced: 163 us -> 160 us
  Pallas kernels: 160 us -> 157 us
    pallas_call x1, Pallas kernels: 160 us -> 157 us  [on_device(): pl.pallas_call(functools.partial(kernel, side, cap), out_shape=jax.ShapeD...]
where the time goes in v4:
time: 162 us; the launch traced here: 160 us
  Pallas kernels  157 us (97%)
  local copies, waits for them, and re-layouts  3.04 us (2%)
    pallas_call x1, Pallas kernels, on_device(): pl.pallas_call(functools.partial(kernel, side, cap), out_shape=jax.ShapeD...  157 us

profile of v4, /device:TPU:515, one launch (start us, length us, event | category | flops | bytes accessed | tf_op | source)
XLA Modules:
  0.0 159.9 jit_solution(7911765891394988578)
XLA Ops:
  0.0 0.0 copy-start.1
  0.0 0.7 copy-done.1
  0.7 0.0 copy-start
  0.7 0.7 copy-done
  1.4 0.0 copy-start.2
  1.4 0.7 copy-done.2
  2.1 156.9 %shard_map.73 = bf16[512,1024]{1,0:T(8,128)(2,1)S(1)} custom-call(bf16[512,1024]{1,0:T(8,128)(2,1)} %tok_hbm.1, f32[1,2048]{1,0:T(1,128)S(1)} %bitcast.3, s32[2,512]{1,0:T(2,128)S(1)} %bitcast.4, f32[2,512]{1,0:T(2,128)S(1)} %bitcast.5, bf16[1,2048,256]{2,1,0:T(8,128)(2,1)} %gate_hbm.1, bf16[1,2048,256]{2,1,0:T(8,128)(2,1)} %up_hbm.1, ...), custom_call_target="tpu_custom_call" | custom-call | tf_op jit(solution)/shard_map/pallas_call | solution.py:370
  158.9 1.0 copy.9
Async XLA Ops:
  0.0 0.7 copy-start.1
  0.7 0.7 copy-start
  1.4 0.7 copy-start.2

commit v5 on v4

--- a/solution.py
+++ b/solution.py
@@ -22,7 +22,7 @@
     side, cap,
     tok_hbm, gain, ids, wts, gate_hbm, up_hbm, down_hbm, out,
     tok, wg, wu, wd, snd, rl1, rcv, res, rl2, back, normed, acc, posr, wts_hi_lo,
-    s_w, r_w, l_w, l_t, go, s_a, s_b, s_c, s_d, r1, r2, r3, r3_last, r4,
+    s_w, r_w, l_w, l_t, go, known, s_a, s_b, s_c, s_d, r1, r2, r3, r3_last, r4,
 ):
     S = side
     half_side = S // 2
@@ -50,10 +50,14 @@
     tok_copy.start()
 
     barrier = pltpu.get_barrier_semaphore()
-    for d in range(1, S):
-        pl.semaphore_signal(barrier, inc=1, device_id={"ep": at(d, 0), "tp": c}, device_id_type=MESH)
-        pl.semaphore_signal(barrier, inc=1, device_id={"ep": at(0, d), "tp": c}, device_id_type=MESH)
-    pl.semaphore_signal(barrier, inc=1, device_id={"ep": ep, "tp": 1 - c}, device_id_type=MESH)
+
+    @pl.when(c == 1)
+    def _():
+        for d in range(1, S):
+            for h in range(2):
+                pl.semaphore_signal(barrier, inc=1, device_id={"ep": at(d, 0), "tp": h}, device_id_type=MESH)
+                pl.semaphore_signal(barrier, inc=1, device_id={"ep": at(0, d), "tp": h}, device_id_type=MESH)
+        pl.semaphore_signal(barrier, inc=1, device_id={"ep": ep, "tp": 0}, device_id_type=MESH)
 
     weights = ((gate_hbm, wg), (up_hbm, wu), (down_hbm, wd))
     row = lax.broadcasted_iota(jnp.int32, (128, tok_rows), 0)
@@ -88,8 +92,8 @@
     def first_axis(core, k):
         return (core + k) % 2
 
-    def coords(j, k):
-        f = first_axis(c, k)
+    def coords(j, k, core=c):
+        f = first_axis(core, k)
         t = (j + (1 - 2 * f) * k + S) % S
         return t, j * (1 - f) + t * f, j * f + t * (1 - f)
 
@@ -118,17 +122,17 @@
             t, dx, dy = coords(j, k)
             p = dx % 2
             q = dx // 2
-            now = (p != c) if crossing else (p == c)
+            now = (p == 0) if crossing else (p == 1)
             if j == 0:
                 @pl.when(now & (t != 0))
                 def _():
                     send(snd.at[k, j], rcv.at[k, q, c], s_a, r2.at[k], at(dx, dy), p)
 
-                if not crossing:
+                if crossing:
                     @pl.when((t == 0) & (c == 1))
                     def _():
                         send(snd.at[k, j], rcv.at[k, q, c], s_a, r2.at[k], ep, 0)
-
+                else:
                     @pl.when((t == 0) & (c == 0))
                     def _():
                         rcv[0, 0, 0] = snd[0, 0]
@@ -136,13 +140,13 @@
                 if not crossing:
                     @pl.when(t != 0)
                     def _():
-                        send(snd.at[k, j], rl1.at[k, j], s_a, r1.at[k], at(j * (1 - f), j * f), c)
+                        send(snd.at[k, j], rl1.at[c, k, j], s_a, r1.at[c, k], at(j * (1 - f), j * f), 1)
 
                 @pl.when(now & (t == 0))
                 def _():
                     send(snd.at[k, j], rcv.at[k, q, c], s_a, r2.at[k], at(dx, dy), p)
 
-    def dispatch_same(k):
+    def dispatch_first(k):
         dispatch(k, False)
 
     def dispatch_crossing(k):
@@ -161,17 +165,21 @@
             def _():
                 wait_blocks(sem, ref.at[k], S - 2)
 
-    def relay_dispatch(k):
-        wait_relayed(r1.at[k], rl1, k)
-        f = first_axis(c, k)
+    def relay_half(k, h):
+        wait_relayed(r1.at[h, k], rl1.at[h], k)
+        f = first_axis(h, k)
         for j in range(1, S):
-            t, dx, dy = coords(j, k)
-            p = dx % 2
-            q = dx // 2
+            t, dx, dy = coords(j, k, h)
 
             @pl.when(t != 0)
             def _():
-                send(rl1.at[k, j], rcv.at[k, q, c], s_b, r2.at[k], at(t * f, t * (1 - f)), p)
+                send(rl1.at[h, k, j], rcv.at[k, dx // 2, h], s_b, r2.at[k], at(t * f, t * (1 - f)), dx % 2)
+
+    def relay_dispatch(k):
+        @pl.when(c == 1)
+        def _():
+            for h in range(2):
+                relay_half(k, h)
 
     def send_relayed(k, j, src, chip, core):
         @pl.when(k == S - 1)
@@ -293,15 +301,28 @@
 
     tok_copy.wait()
     gather(0)
-    pl.semaphore_wait(barrier, 2 * (S - 1) + 1)
-    pl.semaphore_signal(go, inc=1, device_id={"ep": ep, "tp": 1 - c}, device_id_type=MESH)
-    dispatch_same(0)
-    loop(1, S, gather, dispatch_same)
+    pl.semaphore_wait(barrier, 2 * (S - 1) + 1 - c)
+
+    @pl.when(c == 0)
+    def _():
+        pl.semaphore_signal(go, inc=1, device_id={"ep": ep, "tp": 1}, device_id_type=MESH)
+
+    dispatch_first(0)
+    loop(1, S, gather, dispatch_first)
+    pl.semaphore_wait(go, 1)
+
+    @pl.when(c == 1)
+    def _():
+        for d in range(1, S):
+            pl.semaphore_signal(known, inc=1, device_id={"ep": at(d, 0), "tp": 1}, device_id_type=MESH)
+            pl.semaphore_signal(known, inc=1, device_id={"ep": at(0, d), "tp": 1}, device_id_type=MESH)
+        pl.semaphore_wait(known, 2 * (S - 1))
+        pl.semaphore_signal(go, inc=1, device_id={"ep": ep, "tp": 0}, device_id_type=MESH)
+
+    loop(0, S, dispatch_crossing)
     for i, (src, dst) in enumerate(weights):
         send(src.at[0], dst.at[c], s_w.at[i], r_w.at[i], ep, 1 - c)
         pltpu.make_async_copy(src.at[0], dst.at[c], l_w.at[i]).start()
-    pl.semaphore_wait(go, 1)
-    loop(0, S, dispatch_crossing)
     weight_table()
     acc[...] = jnp.zeros_like(acc)
     ahead = min(3, S)
@@ -349,8 +370,13 @@
         @pl.when(c != 0)
         def _():
             all_sent(sem, blocks_sent)
-    for sem in (s_b, s_d):
-        all_sent(sem, relayed)
+    all_sent(s_d, relayed)
+
+    @pl.when(c == 1)
+    def _():
+        for h in range(2):
+            all_sent(s_b, relayed)
+
     for i, (src, dst) in enumerate(weights):
         wait(s_w.at[i], dst.at[c])
 
@@ -378,7 +404,7 @@
             pltpu.VMEM((2, width, part), BF16),
             pltpu.VMEM((2, 2 * part, half), BF16),
             pltpu.VMEM((S, S) + block, BF16),
-            pltpu.VMEM((S, S) + block, BF16),
+            pltpu.VMEM((2, S, S) + block, BF16),
             pltpu.VMEM((S, S // 2, 2) + block, BF16),
             pltpu.VMEM((S, S // 2, 2) + block, BF16),
             pltpu.VMEM((S, S) + block, BF16),
@@ -387,9 +413,9 @@
             pltpu.VMEM((tok_rows, half), F32),
             pltpu.VMEM((8, tok_rows), F32),
             pltpu.VMEM((tok_rows, 128), F32),
-            dma((3,)), dma((3,)), dma((3,)), dma, pltpu.SemaphoreType.REGULAR,
+            dma((3,)), dma((3,)), dma((3,)), dma, pltpu.SemaphoreType.REGULAR, pltpu.SemaphoreType.REGULAR,
             dma, dma, dma, dma,
-            dma((S,)), dma((S,)), dma((S,)), dma((S,)), dma((S, 2)),
+            dma((2, S)), dma((S,)), dma((S,)), dma((S,)), dma((S, 2)),
         ],
         compiler_params=pltpu.CompilerParams(
             collective_id=0, has_side_effects=True, vmem_limit_bytes=52 * 2**20

time: 162 us -> 159 us (0.981); the launches traced: 160 us -> 159 us
  no operation moved by 1% of the time
where the time goes in v5:
time: 159 us
  Pallas kernels  156 us (98%)
  local copies, waits for them, and re-layouts  3.04 us (2%)
    pallas_call x1, Pallas kernels, on_device(): pl.pallas_call(functools.partial(kernel, side, cap), out_shape=jax.ShapeD...  156 us

profile of v5, /device:TPU:515, one launch (start us, length us, event | category | flops | bytes accessed | tf_op | source)
XLA Modules:
  0.0 159.0 jit_solution(1474812334102873559)
XLA Ops:
  0.0 0.0 copy-start.1
  0.0 0.7 copy-done.1
  0.7 0.0 copy-start
  0.7 0.7 copy-done
  1.4 0.0 copy-start.2
  1.4 0.7 copy-done.2
  2.1 155.9 %shard_map.73 = bf16[512,1024]{1,0:T(8,128)(2,1)S(1)} custom-call(bf16[512,1024]{1,0:T(8,128)(2,1)} %tok_hbm.1, f32[1,2048]{1,0:T(1,128)S(1)} %bitcast.3, s32[2,512]{1,0:T(2,128)S(1)} %bitcast.4, f32[2,512]{1,0:T(2,128)S(1)} %bitcast.5, bf16[1,2048,256]{2,1,0:T(8,128)(2,1)} %gate_hbm.1, bf16[1,2048,256]{2,1,0:T(8,128)(2,1)} %up_hbm.1, ...), custom_call_target="tpu_custom_call" | custom-call | tf_op jit(solution)/shard_map/pallas_call | solution.py:396
  158.0 1.0 copy.9
Async XLA Ops:
  0.0 0.7 copy-start.1
  0.7 0.7 copy-start
  1.4 0.7 copy-start.2

commit v6 on v5

--- a/solution.py
+++ b/solution.py
@@ -26,6 +26,7 @@
 ):
     S = side
     half_side = S // 2
+    far_first = sorted(range(S), key=lambda j: -min(j, S - j))
     c = lax.axis_index("tp")
     ep = lax.axis_index("ep")
     y = ep // S
@@ -118,7 +119,7 @@
 
     def dispatch(k, crossing):
         f = first_axis(c, k)
-        for j in range(S):
+        for j in far_first:
             t, dx, dy = coords(j, k)
             p = dx % 2
             q = dx // 2
@@ -168,7 +169,7 @@
     def relay_half(k, h):
         wait_relayed(r1.at[h, k], rl1.at[h], k)
         f = first_axis(h, k)
-        for j in range(1, S):
+        for j in far_first[:-1]:
             t, dx, dy = coords(j, k, h)
 
             @pl.when(t != 0)

time: 159 us -> 160 us (level)
  no operation moved by 1% of the time
where the time goes in v6:
time: 160 us; the launch traced here: 159 us
  Pallas kernels  156 us (98%)
  local copies, waits for them, and re-layouts  3.04 us (2%)
    pallas_call x1, Pallas kernels, on_device(): pl.pallas_call(functools.partial(kernel, side, cap), out_shape=jax.ShapeD...  156 us

profile of v6, /device:TPU:515, one launch (start us, length us, event | category | flops | bytes accessed | tf_op | source)
XLA Modules:
  0.0 158.9 jit_solution(826436239151617274)
XLA Ops:
  0.0 0.0 copy-start.1
  0.0 0.7 copy-done.1
  0.7 0.0 copy-start
  0.7 0.7 copy-done
  1.4 0.0 copy-start.2
  1.4 0.7 copy-done.2
  2.1 155.9 %shard_map.73 = bf16[512,1024]{1,0:T(8,128)(2,1)S(1)} custom-call(bf16[512,1024]{1,0:T(8,128)(2,1)} %tok_hbm.1, f32[1,2048]{1,0:T(1,128)S(1)} %bitcast.3, s32[2,512]{1,0:T(2,128)S(1)} %bitcast.4, f32[2,512]{1,0:T(2,128)S(1)} %bitcast.5, bf16[1,2048,256]{2,1,0:T(8,128)(2,1)} %gate_hbm.1, bf16[1,2048,256]{2,1,0:T(8,128)(2,1)} %up_hbm.1, ...), custom_call_target="tpu_custom_call" | custom-call | tf_op jit(solution)/shard_map/pallas_call | solution.py:397
  157.9 1.0 copy.9
Async XLA Ops:
  0.0 0.7 copy-start.1
  0.7 0.7 copy-start
  1.4 0.7 copy-start.2
